TPU v7x, 128 devices: a whole 4x4x4 slice. The times are simulated.
128 devices in a mesh: ep: 128 (over z, y, x, core).
Axes of the slice: x: 4, y: 4, z: 4, core: 2. Of those that a mesh axis runs over, the one named last changes fastest.
Arguments:
- tokens: bfloat16 [2048, 2048], P('ep'), may hold values from -6 to 6
- lengths: int32 [2048], P('ep'), may hold values from 1 to 1024, 1048576 in all
- cache_keys: bfloat16 [2048, 1024, 128], P('ep'), may hold values from -6 to 6
- cache_values: bfloat16 [2048, 1024, 128], P('ep'), may hold values from -6 to 6
- mix_gain: float32 [2048], replicated, may hold values from 0.1 to 1.9
- mix_out_gain: float32 [2048], replicated, may hold values from 0.1 to 1.9
- ffn_gain: float32 [2048], replicated, may hold values from 0.1 to 1.9
- ffn_out_gain: float32 [2048], replicated, may hold values from 0.1 to 1.9
- query_weight: bfloat16 [2048, 2048], P(None, 'ep'), may hold values from -0.125 to 0.125
- key_weight: bfloat16 [2048, 128], replicated, may hold values from -0.125 to 0.125
- value_weight: bfloat16 [2048, 128], replicated, may hold values from -0.125 to 0.125
- head_bias: float32 [32], replicated, may hold values from -8 to -2
- output_weight: bfloat16 [2048, 2048], P(None, 'ep'), may hold values from -0.125 to 0.125
- routes: int32 [2048, 6], P('ep'), may hold values from 0 to 127, all different within a row; in each aligned block of 16 rows (0 to 15, 16 to 31, ...) at most 2 rows name the same one
- route_weights: float32 [2048, 6], P('ep'), may hold values from 0.1 to 1
- expert_gate: bfloat16 [128, 2048, 512], P('ep'), may hold values from -0.125 to 0.125
- expert_up: bfloat16 [128, 2048, 512], P('ep'), may hold values from -0.125 to 0.125
- expert_down: bfloat16 [128, 512, 2048], P('ep'), may hold values from -0.25 to 0.25
- shared_gate: bfloat16 [2048, 512], replicated, may hold values from -0.125 to 0.125
- shared_up: bfloat16 [2048, 512], replicated, may hold values from -0.125 to 0.125
- shared_down: bfloat16 [512, 2048], replicated, may hold values from -0.25 to 0.25
Outputs:
- layer_out: bfloat16 [2048, 2048], P('ep')
- new_keys: bfloat16 [2048, 128], P('ep')
- new_values: bfloat16 [2048, 128], P('ep')
Inputs may be any that keep to these rules, and one draw needn't show every extreme that they name: `routes`: each row names 6 different experts. Among the rows of one device no expert is named more than 2 times, a bound that some block reaches in some device's rows. `lengths`: the new token stands at this position; cache entries at this position and after are unused. Some sequence has exactly 1024.
All inputs are finite; a program needn't handle non-finite values. No bound on the sum of `lengths` on one device may be relied on, other than what follows from the above.
Results may differ from a plain program's by a relative error of at most 0.013.
Values may be sent and summed in bfloat16 or wider, within the bound.
No kernel may reach another device: no remote copies, remote signals or barrier semaphores. Data moves between devices by JAX's collectives and lax.ppermute only.
A program may use at most 128 MiB of HBM per device.

v0:
```python
import math
import jax
import jax.numpy as jnp
from jax import lax
from jax.sharding import PartitionSpec as P

HD = 64


def rms_scale(rows, gain):
    return rows * lax.rsqrt(jnp.mean(rows * rows, axis=-1, keepdims=True) + 1e-06) * gain


def later_sums(values):
    seqs, kv_heads, group, span = values.shape
    width = math.gcd(span, 128)
    count = span // width
    blocked = values.reshape(seqs, kv_heads, group, count, width)
    inner_pos = jnp.arange(width)
    upper = (inner_pos[:, None] > inner_pos[None, :]).astype(jnp.float32)
    inside = jnp.einsum("skgbj,ji->skgbi", blocked, upper, precision=lax.Precision.HIGHEST)
    totals = jnp.sum(blocked, axis=4)
    block_pos = jnp.arange(count)
    beyond = (block_pos[:, None] > block_pos[None, :]).astype(jnp.float32)
    carried = jnp.einsum("skgc,cb->skgb", totals, beyond, precision=lax.Precision.HIGHEST)
    return (inside + carried[..., None]).reshape(seqs, kv_heads, group, span)


def body(
    tokens,
    lengths,
    cache_keys,
    cache_values,
    mix_gain,
    mix_out_gain,
    ffn_gain,
    ffn_out_gain,
    query_weight,
    key_weight,
    value_weight,
    head_bias,
    output_weight,
    routes,
    route_weights,
    expert_gate,
    expert_up,
    expert_down,
    shared_gate,
    shared_up,
    shared_down,
):
    resid = tokens.astype(jnp.float32)
    normed = rms_scale(resid, mix_gain).astype(jnp.bfloat16)
    new_keys = jnp.dot(normed, key_weight, preferred_element_type=jnp.float32).astype(jnp.bfloat16)
    new_values = jnp.dot(normed, value_weight, preferred_element_type=jnp.float32).astype(
        jnp.bfloat16
    )
    queries = jnp.dot(
        normed,
        lax.all_gather(query_weight, "ep", axis=1, tiled=True),
        preferred_element_type=jnp.float32,
    ).astype(jnp.bfloat16)
    seqs, span, width = cache_keys.shape
    kv_heads = width // HD
    heads = queries.shape[1] // HD
    group = heads // kv_heads
    q_heads = queries.reshape(seqs, kv_heads, group, HD)
    k_heads = cache_keys.reshape(seqs, span, kv_heads, HD)
    v_heads = cache_values.reshape(seqs, span, kv_heads, HD)
    scores = jnp.einsum(
        "skgd,slkd->skgl", q_heads, k_heads, preferred_element_type=jnp.float32
    ) * HD ** (-0.5)
    scores = scores + head_bias.reshape(kv_heads, group)[None, :, :, None]
    valid = (jnp.arange(span)[None, :] < lengths[:, None])[:, None, None, :]
    log_beta = jax.nn.log_sigmoid(scores)
    log_keep = jnp.where(valid, log_beta - scores, 0.0)
    after = later_sums(log_keep)
    stick = jnp.where(valid, jnp.exp(log_beta + after), 0.0).astype(jnp.bfloat16)
    attended = jnp.einsum("skgl,slkd->skgd", stick, v_heads, preferred_element_type=jnp.float32)
    attended = attended.astype(jnp.bfloat16).reshape(seqs, heads * HD)
    mixed = jnp.dot(
        attended,
        lax.all_gather(output_weight, "ep", axis=1, tiled=True),
        preferred_element_type=jnp.float32,
    ).astype(jnp.bfloat16)
    resid1 = resid + rms_scale(mixed.astype(jnp.float32), mix_out_gain)
    ffn_in = rms_scale(resid1, ffn_gain).astype(jnp.bfloat16)
    devices = lax.axis_size("ep")
    top = routes.shape[1]
    experts = devices * expert_gate.shape[0]
    capacity = 2 * ((seqs * top + devices - 1) // devices)
    flat = routes.reshape(-1)
    onehot = (flat[:, None] == jnp.arange(experts)[None, :]).astype(jnp.float32)
    assign_pos = jnp.arange(flat.shape[0])
    lower = (assign_pos[:, None] > assign_pos[None, :]).astype(jnp.float32)
    earlier = jnp.dot(lower, onehot, precision=lax.Precision.HIGHEST)
    rank = jnp.sum(earlier * onehot, axis=1).astype(jnp.int32)
    slot = flat * capacity + rank
    placed = slot.reshape(seqs, top)[:, :, None] == jnp.arange(experts * capacity)[None, None, :]
    dispatch = jnp.sum(placed.astype(jnp.float32), axis=1).astype(jnp.bfloat16)
    outgoing = jnp.einsum("sc,sd->cd", dispatch, ffn_in, preferred_element_type=jnp.float32)
    outgoing = outgoing.astype(jnp.bfloat16).reshape(experts, capacity, ffn_in.shape[1])
    shared_hidden = (
        jax.nn.silu(jnp.dot(ffn_in, shared_gate, preferred_element_type=jnp.float32))
        * jnp.dot(ffn_in, shared_up, preferred_element_type=jnp.float32)
    ).astype(jnp.bfloat16)
    shared_out = jnp.dot(shared_hidden, shared_down, preferred_element_type=jnp.float32)
    incoming = lax.all_to_all(outgoing, "ep", split_axis=0, concat_axis=0, tiled=True)
    sources, count, features = incoming.shape
    rows = incoming.reshape(sources * count, features)
    hidden = (
        jax.nn.silu(jnp.dot(rows, expert_gate[0], preferred_element_type=jnp.float32))
        * jnp.dot(rows, expert_up[0], preferred_element_type=jnp.float32)
    ).astype(jnp.bfloat16)
    result = jnp.dot(hidden, expert_down[0], preferred_element_type=jnp.float32).astype(
        jnp.bfloat16
    )
    returned = lax.all_to_all(
        result.reshape(sources, count, features), "ep", split_axis=0, concat_axis=0, tiled=True
    )
    picked = jnp.take(returned.reshape(experts * capacity, -1), slot, axis=0)
    routed = jnp.sum(
        picked.astype(jnp.float32).reshape(seqs, top, -1) * route_weights[:, :, None], axis=1
    )
    layer_out = (resid1 + rms_scale(routed + shared_out, ffn_out_gain)).astype(jnp.bfloat16)
    return (layer_out, new_keys, new_values)


def solution(mesh):
    in_specs = (
        P("ep", None),
        P("ep"),
        P("ep", None, None),
        P("ep", None, None),
        P(),
        P(),
        P(),
        P(),
        P(None, "ep"),
        P(),
        P(),
        P(),
        P(None, "ep"),
        P("ep", None),
        P("ep", None),
        P("ep", None, None),
        P("ep", None, None),
        P("ep", None, None),
        P(),
        P(),
        P(),
    )
    out_specs = (P("ep", None), P("ep", None), P("ep", None))
    return jax.shard_map(body, mesh=mesh, in_specs=in_specs, out_specs=out_specs, check_vma=False)
```

profile of v0, /device:TPU:1, one launch (start us, length us, event | category | flops | bytes accessed | tf_op | source)
XLA Modules:
  0.0 238.4 jit_solution(5669032476505502544)
XLA Ops:
  7.2 0.0 copy-start
  7.2 0.0 all-gather.3.cloned.1.call-start
  7.2 0.7 all-gather.3.cloned.1.call-update
  7.9 0.0 all-gather.5.cloned.1.call-start
  8.0 0.7 all-gather.5.cloned.1.call-update
  8.7 0.7 add.115
  9.4 6.4 %copy.43 = bf16[16,1024,128]{1,2,0:T(8,128)(2,1)} copy(bf16[16,1024,128]{2,1,0:T(8,128)(2,1)} %param.23) | data formatting | bytes 8388608 | tf_op args[2]
  15.8 6.5 %copy.46 = bf16[16,1024,128]{1,2,0:T(8,128)(2,1)} copy(bf16[16,1024,128]{2,1,0:T(8,128)(2,1)} %param.24) | data formatting | bytes 8388608 | tf_op args[3]
  22.3 0.0 copy-done.9
  22.3 0.1 copy.47
  22.4 0.1 reshape.156
  22.5 0.3 fusion.13
  22.8 0.1 convert_element_type.88
  22.9 0.1 copy.49
  23.0 0.1 convert_reduce_fusion
  23.1 0.0 copy-done.1
  23.1 0.1 fusion.26
  23.2 0.0 copy-done.11
  23.2 0.1 iota_compare_fusion.2
  23.3 61.0 %all-gather.3.cloned.1.call-done = bf16[2048,2048]{0,1:T(8,128)(2,1)} async-done(((bf16[2048,16]{0,1:T(8,128)(2,1)}), bf16[2048,2048]{0,1:T(8,128)(2,1)}) %all-gather.3.cloned.1.call-update) | async-done | bytes 8388624 | tf_op jit(solution)/shard_map/all_gather | solution.py:60
  84.3 0.0 copy-done.5
  84.3 5.6 %convolution_convert_fusion.3 = bf16[16,2048]{1,0:T(8,128)(2,1)S(1)} fusion(bf16[2048,2048]{0,1:T(8,128)(2,1)} %all-gather.3.cloned.1.call-done, bf16[16,2048]{1,0:T(8,128)(2,1)S(1)} %copy-done.1, f32[2048]{0:T(1024)S(1)} %copy-done.5, f32[16]{0:T(128)S(1)} %add_rsqrt_fusion.3), kind=kOutput, calls=%fused_computation.7 | convolution fusion | flops 134381568 | bytes 8527936 | tf_op jit(solution)/shard_map/dot_general | solution.py:58
  90.0 0.2 reshape.150
  90.2 5.3 %subtract_select_fusion = (f32[16,2,16,1024]{3,2,1,0:T(8,128)S(1)}, f32[16,2,16,1024]{3,2,1,0:T(8,128)}) fusion(f32[2,16]{1,0:T(2,128)S(1)} %add.115, pred[16,1024]{1,0:T(8,128)(4,1)S(1)} %iota_compare_fusion.2, bf16[16,2,16,64]{3,2,1,0:T(8,128)(2,1)S(1)} %reshape.150, bf16[16,1024,2,64]{1,3,2,0:T(8,128)(2,1)} %bitcast.64), kind=kOutput, calls=%fused_computation.15 | convolution fusion | flops 73400320 | bytes 8470656 | tf_op jit(solution)/shard_map/skgd,slkd->skgl/dot_general | solution.py:70
  95.5 1.8 copy.55
  97.2 2.2 reduce_sum.73
  99.4 0.2 fusion.40
  99.7 4.1 %convolution_add_fusion.1 = f32[16,2,16,8,128]{4,3,2,1,0:T(8,128)} fusion(f32[16,2,16,8,128]{4,3,2,1,0:T(8,128)} %bitcast.62, f32[16,2,16,8]{3,2,1,0:T(8,128)S(1)} %fusion.40), kind=kOutput, calls=%fused_computation.17 | convolution fusion | flops 805847040 | bytes 4210688 | tf_op jit(solution)/shard_map/skgbj,ji->skgbi/dot_general | solution.py:21
  103.8 2.7 %reshape.153 = f32[16,2,16,1024]{3,2,1,0:T(8,128)} reshape(f32[16,2,16,8,128]{4,3,2,1,0:T(8,128)} %convolution_add_fusion.1) | data formatting | bytes 4194304 | tf_op jit(solution)/shard_map/reshape | solution.py:26
  106.5 5.4 %convolution_convert_fusion.4 = bf16[16,2,16,64]{3,2,1,0:T(8,128)(2,1)S(1)} fusion(bf16[16,1024,2,64]{1,3,2,0:T(8,128)(2,1)} %bitcast.63, f32[16,2,16,1024]{3,2,1,0:T(8,128)} %reshape.153, f32[16,2,16,1024]{3,2,1,0:T(8,128)} %get-tuple-element.6, f32[2,16]{1,0:T(2,128)S(1)} %add.115, pred[16,1024]{1,0:T(8,128)(4,1)S(1)} %iota_compare_fusion.2), kind=kOutput, calls=%fused_computation.20 | convolution fusion | flops 73957376 | bytes 8470656 | tf_op jit(solution)/shard_map/skgl,slkd->skgd/dot_general | solution.py:79
  111.9 0.2 reshape.155
  112.1 0.0 copy-start.6
  112.1 0.0 copy-start.7
  112.1 42.4 %all-gather.5.cloned.1.call-done = bf16[2048,2048]{0,1:T(8,128)(2,1)} async-done(((bf16[2048,16]{0,1:T(8,128)(2,1)}), bf16[2048,2048]{0,1:T(8,128)(2,1)}) %all-gather.5.cloned.1.call-update) | async-done | bytes 8388624 | tf_op jit(solution)/shard_map/all_gather | solution.py:83
  154.5 5.8 %multiply_reduce_fusion.3 = (f32[16]{0:T(128)S(1)}, f32[16,2048]{1,0:T(8,128)S(1)}) fusion(bf16[16,2048]{1,0:T(8,128)(2,1)S(1)} %reshape.155, bf16[2048,2048]{0,1:T(8,128)(2,1)} %all-gather.5.cloned.1.call-done), kind=kOutput, calls=%fused_computation.47 | convolution fusion | flops 134348784 | bytes 8585280 | tf_op jit(solution)/shard_map/dot_general | solution.py:81
  160.3 0.0 copy-done.6
  160.3 0.2 multiply_reduce_fusion.2
  160.5 0.0 copy-done.7
  160.5 0.1 multiply_convert_fusion
  160.6 0.4 convolution_convert_fusion.1
  161.1 0.0 copy-start.10
  161.1 1.5 reshape.157
  162.6 5.4 %all-to-all-start = ((bf16[128,2,2048]{2,1,0:T(2,128)(2,1)}), bf16[128,2,2048]{2,1,0:T(2,128)(2,1)S(1)}, u32[]{:S(2)}, u32[]{:S(2)}) async-start(bf16[128,2,2048]{2,1,0:T(2,128)(2,1)} %reshape.157), calls=%async_computation | async-start | bytes 2097152 | tf_op jit(solution)/shard_map/all_to_all | solution.py:108
  168.0 0.1 mul.150
  168.1 0.1 copy.50
  168.2 19.0 %all-to-all-done = bf16[128,2,2048]{2,1,0:T(2,128)(2,1)S(1)} async-done(((bf16[128,2,2048]{2,1,0:T(2,128)(2,1)}), bf16[128,2,2048]{2,1,0:T(2,128)(2,1)S(1)}, u32[]{:S(2)}, u32[]{:S(2)}) %all-to-all-start) | async-done | bytes 1048608 | tf_op jit(solution)/shard_map/all_to_all | solution.py:108
  187.2 1.2 reshape.158
  188.4 3.5 %fusion.5 = f32[256,512]{1,0:T(8,128)} fusion(bf16[256,2048]{1,0:T(8,128)(2,1)} %reshape.158, bf16[1,2048,512]{2,1,0:T(8,128)(2,1)} %param.36), kind=kOutput, calls=%fused_computation.12 | convolution fusion | flops 536870912 | bytes 3670016 | tf_op jit(solution)/shard_map/dot_general | solution.py:112
  191.9 0.0 copy-done
  191.9 4.0 %convolution_convert_fusion = bf16[256,2048]{1,0:T(8,128)(2,1)} fusion(bf16[1,512,2048]{2,1,0:T(8,128)(2,1)S(1)} %copy-done, bf16[256,2048]{1,0:T(8,128)(2,1)S(1)} %copy-done.2, bf16[1,2048,512]{2,1,0:T(8,128)(2,1)} %param.37, f32[256,512]{1,0:T(8,128)} %fusion.5), kind=kOutput, calls=%fused_computation.2 | convolution fusion | flops 1075052544 | bytes 6815744 | tf_op jit(solution)/shard_map/dot_general | solution.py:115
  195.9 2.6 %reshape.159 = bf16[128,2,2048]{2,1,0:T(2,128)(2,1)} reshape(bf16[256,2048]{1,0:T(8,128)(2,1)} %convolution_convert_fusion) | data formatting | bytes 2097152 | tf_op jit(solution)/shard_map/reshape | solution.py:119
  198.5 5.4 %all-to-all-start.1 = ((bf16[128,2,2048]{2,1,0:T(2,128)(2,1)}), bf16[128,2,2048]{2,1,0:T(2,128)(2,1)}, u32[]{:S(2)}, u32[]{:S(2)}) async-start(bf16[128,2,2048]{2,1,0:T(2,128)(2,1)} %reshape.159), calls=%async_computation.1 | async-start | bytes 2097152 | tf_op jit(solution)/shard_map/all_to_all | solution.py:118
  204.0 0.8 convolution_convert_fusion.5
  204.9 0.8 convolution_convert_fusion.6
  205.7 2.0 fusion.52
  207.7 15.3 %all-to-all-done.1 = bf16[128,2,2048]{2,1,0:T(2,128)(2,1)} async-done(((bf16[128,2,2048]{2,1,0:T(2,128)(2,1)}), bf16[128,2,2048]{2,1,0:T(2,128)(2,1)}, u32[]{:S(2)}, u32[]{:S(2)}) %all-to-all-start.1) | async-done | bytes 1048608 | tf_op jit(solution)/shard_map/all_to_all | solution.py:118
  223.0 1.5 reshape.160
  224.5 1.6 gather_fusion
  226.1 1.1 gather.7
  227.2 0.6 multiply_reduce_fusion
  227.8 0.0 copy-start.8
  227.8 3.1 %multiply_reduce_fusion.1 = (f32[16]{0:T(128)S(1)}, f32[16,2048]{1,0:T(8,128)S(1)}) fusion(f32[16,2048]{1,0:T(8,128)S(1)} %multiply_reduce_fusion, bf16[512,2048]{1,0:T(8,128)(2,1)} %param.41, bf16[16,2048]{1,0:T(8,128)(2,1)S(1)} %multiply_convert_fusion, bf16[2048,512]{1,0:T(8,128)(2,1)} %param.40, f32[16,512]{1,0:T(8,128)S(1)} %fusion.52), kind=kOutput, calls=%fused_computation.44 | convolution fusion | flops 67256304 | bytes 4554816 | tf_op jit(solution)/shard_map/dot_general | solution.py:107
  230.9 0.0 copy-done.8
  230.9 0.7 add_convert_fusion
  (20 shorter events, 0.1 us)
Async XLA Ops:
  7.2 184.7 %copy-start = (bf16[1,512,2048]{2,1,0:T(8,128)(2,1)S(1)}, bf16[1,512,2048]{2,1,0:T(8,128)(2,1)}, u32[]{:S(2)}) copy-start(bf16[1,512,2048]{2,1,0:T(8,128)(2,1)} %param.38) | copy-start | bytes 6291460
  7.2 77.1 %all-gather.3.cloned.1.call-start = ((), (), s32[]{:S(2)}) async-start(), calls=%async_computation.2 | async-start | bytes 8454144 | tf_op jit(solution)/shard_map/all_gather | solution.py:60
  7.9 146.6 %all-gather.5.cloned.1.call-start = ((), (), s32[]{:S(2)}) async-start(), calls=%async_computation.3 | async-start | bytes 8454144 | tf_op jit(solution)/shard_map/all_gather | solution.py:83
  15.8 6.5 %copy-start.9 = (s32[16,6]{0,1:T(8,128)S(1)}, s32[16,6]{0,1:T(8,128)}, u32[]{:S(2)}) copy-start(s32[16,6]{0,1:T(8,128)} %param.34) | copy-start | bytes 1156
  15.8 7.3 %copy-start.1 = (bf16[16,2048]{1,0:T(8,128)(2,1)S(1)}, bf16[16,2048]{1,0:T(8,128)(2,1)}, u32[]{:S(2)}) copy-start(bf16[16,2048]{1,0:T(8,128)(2,1)} %param.21) | copy-start | bytes 196612
  15.8 7.4 %copy-start.11 = (s32[16]{0:T(128)S(1)}, s32[16]{0:T(128)}, u32[]{:S(2)}) copy-start(s32[16]{0:T(128)} %param.22) | copy-start | bytes 196
  15.8 68.5 %copy-start.5 = (f32[2048]{0:T(1024)S(1)}, f32[2048]{0:T(1024)}, u32[]{:S(2)}) copy-start(f32[2048]{0:T(1024)} %param.25) | copy-start | bytes 24580
  112.1 48.2 %copy-start.6 = (f32[2048]{0:T(1024)S(1)}, f32[2048]{0:T(1024)}, u32[]{:S(2)}) copy-start(f32[2048]{0:T(1024)} %param.26) | copy-start | bytes 24580
  112.1 48.4 %copy-start.7 = (f32[2048]{0:T(1024)S(1)}, f32[2048]{0:T(1024)}, u32[]{:S(2)}) copy-start(f32[2048]{0:T(1024)} %param.27) | copy-start | bytes 24580
  161.1 7.0 %copy-start.10 = (f32[16,6]{0,1:T(8,128)S(1)}, f32[16,6]{0,1:T(8,128)}, u32[]{:S(2)}) copy-start(f32[16,6]{0,1:T(8,128)} %param.35) | copy-start | bytes 1156
  162.6 24.6 %all-to-all-start = ((bf16[128,2,2048]{2,1,0:T(2,128)(2,1)}), bf16[128,2,2048]{2,1,0:T(2,128)(2,1)S(1)}, u32[]{:S(2)}, u32[]{:S(2)}) async-start(bf16[128,2,2048]{2,1,0:T(2,128)(2,1)} %reshape.157), calls=%async_computation | async-start | bytes 2097152 | tf_op jit(solution)/shard_map/all_to_all | solution.py:108
  188.4 3.5 %copy-start.2 = (bf16[256,2048]{1,0:T(8,128)(2,1)S(1)}, bf16[256,2048]{1,0:T(8,128)(2,1)}, u32[]{:S(2)}) copy-start(bf16[256,2048]{1,0:T(8,128)(2,1)} %reshape.158) | copy-start | bytes 3145732
  195.9 8.1 %copy-start.3 = (bf16[2048,128]{1,0:T(8,128)(2,1)S(1)}, bf16[2048,128]{1,0:T(8,128)(2,1)}, u32[]{:S(2)}) copy-start(bf16[2048,128]{1,0:T(8,128)(2,1)} %param.31) | copy-start | bytes 1572868
  195.9 9.0 %copy-start.4 = (bf16[2048,128]{1,0:T(8,128)(2,1)S(1)}, bf16[2048,128]{1,0:T(8,128)(2,1)}, u32[]{:S(2)}) copy-start(bf16[2048,128]{1,0:T(8,128)(2,1)} %param.30) | copy-start | bytes 1572868
  198.5 24.5 %all-to-all-start.1 = ((bf16[128,2,2048]{2,1,0:T(2,128)(2,1)}), bf16[128,2,2048]{2,1,0:T(2,128)(2,1)}, u32[]{:S(2)}, u32[]{:S(2)}) async-start(bf16[128,2,2048]{2,1,0:T(2,128)(2,1)} %reshape.159), calls=%async_computation.1 | async-start | bytes 2097152 | tf_op jit(solution)/shard_map/all_to_all | solution.py:118
  227.8 3.1 %copy-start.8 = (f32[2048]{0:T(1024)S(1)}, f32[2048]{0:T(1024)}, u32[]{:S(2)}) copy-start(f32[2048]{0:T(1024)} %param.28) | copy-start | bytes 24580
Sparse Core Ops, SparseCore 0:
  11.0 73.3 all-gather.2
  87.3 67.1 all-gather.4
where the time goes:
time: 239 us; the launch traced here: 238 us
  waiting for transfers between devices  139 us (58%)
  matrix products  41.4 us (17%)
  local copies, waits for them, and re-layouts  28.5 us (12%)
  between operations  14.3 us (6%)
  starting transfers between devices  10.9 us (5%)
  other arithmetic  4.18 us (2%)
    all_gather x1, waiting for transfers between devices, body(): lax.all_gather(query_weight, 'ep', axis=1, tiled=True)  61 us
    all_gather x1, waiting for transfers between devices, body(): lax.all_gather(output_weight, 'ep', axis=1, tiled=True)  42.4 us
    all_to_all x1, waiting for transfers between devices, body(): lax.all_to_all(outgoing, 'ep', split_axis=0, concat_axis=0, tiled=True)  19 us
    all_to_all x1, waiting for transfers between devices, body(): lax.all_to_all(result.reshape(sources, count, features), 'ep', split_axis...  15.3 us
    unnamed x29, local copies, waits for them, and re-layouts  14.9 us
    dot_general x1, matrix products, body(): jnp.dot(attended, lax.all_gather(output_weight, 'ep', axis=1, tiled=True)...  5.76 us
    dot_general x1, matrix products, body(): jnp.dot(normed, lax.all_gather(query_weight, 'ep', axis=1, tiled=True), p...  5.65 us
    all_to_all x1, starting transfers between devices, body(): lax.all_to_all(result.reshape(sources, count, features), 'ep', split_axis...  5.44 us
  transfers between devices with their start and end apart: 4, of which 4 were waited for; matrix products, arithmetic and copies ran while one was open for 19% of the time, Pallas kernels for 0%

commit v1 on v0

--- a/solution.py
+++ b/solution.py
@@ -57,7 +57,9 @@
     )
     queries = jnp.dot(
         normed,
-        lax.all_gather(query_weight, "ep", axis=1, tiled=True),
+        jnp.concatenate(
+            lax.all_to_all(jnp.stack([query_weight] * lax.axis_size("ep")), "ep", 0, 0), axis=1
+        ),
         preferred_element_type=jnp.float32,
     ).astype(jnp.bfloat16)
     seqs, span, width = cache_keys.shape

time: 239 us -> 247 us (1.033)
  starting transfers between devices: 10.9 us -> 27 us
  waiting for transfers between devices: 139 us -> 126 us
  local copies, waits for them, and re-layouts: 28.5 us -> 32.9 us
    all_to_all x0 -> x1, waiting for transfers between devices: none -> 87.4 us  [body(): lax.all_to_all(jnp.stack([query_weight] * lax.axis_size('ep')), 'ep', 0, 0)]
    all_gather x1 -> x0, waiting for transfers between devices: 61 us -> none  [body(): lax.all_gather(query_weight, 'ep', axis=1, tiled=True)]
    all_gather x1, waiting for transfers between devices: 42.4 us -> 3.16 us  [body(): lax.all_gather(output_weight, 'ep', axis=1, tiled=True)]
    all_to_all x0 -> x1, starting transfers between devices: none -> 11.9 us  [body(): lax.all_to_all(jnp.stack([query_weight] * lax.axis_size('ep')), 'ep', 0, 0)]
    another operation x0 -> x1, local copies, waits for them, and re-layouts: none -> 5.12 us  [body(): jnp.stack([query_weight] * lax.axis_size('ep'))]
    all_to_all x1, starting transfers between devices: 5.36 us -> 9.62 us  [body(): lax.all_to_all(outgoing, 'ep', split_axis=0, concat_axis=0, tiled=True)]
    unnamed x29 -> x31, local copies, waits for them, and re-layouts: 14.9 us -> 14.8 us
  transfers between devices with their start and end apart: 4 -> 4, of which waited for: 4 -> 4; matrix products, arithmetic and copies ran while one was open for 19% -> 21% of each run, Pallas kernels for 0% -> 0%
where the time goes in v1:
time: 247 us; the launch traced here: 246 us
  waiting for transfers between devices  126 us (51%)
  matrix products  41.8 us (17%)
  local copies, waits for them, and re-layouts  32.9 us (13%)
  starting transfers between devices  27 us (11%)
  between operations  14.3 us (6%)
  other arithmetic  4.18 us (2%)
    all_to_all x1, waiting for transfers between devices, body(): lax.all_to_all(jnp.stack([query_weight] * lax.axis_size('ep')), 'ep', 0, 0)  87.4 us
    all_to_all x1, waiting for transfers between devices, body(): lax.all_to_all(outgoing, 'ep', split_axis=0, concat_axis=0, tiled=True)  19 us
    all_to_all x1, waiting for transfers between devices, body(): lax.all_to_all(result.reshape(sources, count, features), 'ep', split_axis...  15.3 us
    unnamed x31, local copies, waits for them, and re-layouts  14.8 us
    all_to_all x1, starting transfers between devices, body(): lax.all_to_all(jnp.stack([query_weight] * lax.axis_size('ep')), 'ep', 0, 0)  11.9 us
    all_to_all x1, starting transfers between devices, body(): lax.all_to_all(outgoing, 'ep', split_axis=0, concat_axis=0, tiled=True)  9.62 us
    dot_general x1, matrix products, body(): jnp.einsum('skgl,slkd->skgd', stick, v_heads, preferred_element_type=jnp....  5.81 us
    dot_general x1, matrix products, body(): jnp.dot(attended, lax.all_gather(output_weight, 'ep', axis=1, tiled=True)...  5.76 us
  transfers between devices with their start and end apart: 4, of which 4 were waited for; matrix products, arithmetic and copies ran while one was open for 21% of the time, Pallas kernels for 0%

profile of v1, /device:TPU:1, one launch (start us, length us, event | category | flops | bytes accessed | tf_op | source)
XLA Modules:
  0.0 245.9 jit_solution(5244912437778920801)
XLA Ops:
  7.2 0.0 copy-start
  7.2 0.0 all-gather.2.cloned.1.call-start
  7.2 0.7 all-gather.2.cloned.1.call-update
  7.9 5.1 %stack.2 = bf16[128,2048,16]{1,2,0:T(8,128)(2,1)} broadcast(bf16[2048,16]{0,1:T(8,128)(2,1)} %param.29), dimensions={1,2} | broadcast | bytes 8454144 | tf_op jit(solution)/shard_map/stack | solution.py:61
  13.0 11.9 %all-to-all-start = ((bf16[128,2048,16]{1,2,0:T(8,128)(2,1)}), bf16[128,2048,16]{1,2,0:T(8,128)(2,1)}, u32[]{:S(2)}, u32[]{:S(2)}) async-start(bf16[128,2048,16]{1,2,0:T(8,128)(2,1)} %stack.2), calls=%async_computation | async-start | bytes 16777216 | tf_op jit(solution)/shard_map/all_to_all | solution.py:61
  25.0 0.0 copy-done.12
  25.0 0.1 add.115
  25.1 6.4 %copy.44 = bf16[16,1024,128]{1,2,0:T(8,128)(2,1)} copy(bf16[16,1024,128]{2,1,0:T(8,128)(2,1)} %param.23) | data formatting | bytes 8388608 | tf_op args[2]
  31.5 6.4 %copy.47 = bf16[16,1024,128]{1,2,0:T(8,128)(2,1)} copy(bf16[16,1024,128]{2,1,0:T(8,128)(2,1)} %param.24) | data formatting | bytes 8388608 | tf_op args[3]
  37.9 0.0 copy-done.9
  37.9 0.1 copy.48
  38.0 0.1 reshape.166
  38.1 0.3 fusion.13
  38.4 0.1 convert_element_type.88
  38.5 0.1 copy.50
  38.6 0.1 convert_reduce_fusion
  38.7 0.0 copy-done.1
  38.7 0.1 fusion.26
  38.9 0.0 copy-done.11
  38.9 0.1 iota_compare_fusion.2
  38.9 87.4 %all-to-all-done = bf16[128,2048,16]{1,2,0:T(8,128)(2,1)} async-done(((bf16[128,2048,16]{1,2,0:T(8,128)(2,1)}), bf16[128,2048,16]{1,2,0:T(8,128)(2,1)}, u32[]{:S(2)}, u32[]{:S(2)}) %all-to-all-start) | async-done | bytes 8388640 | tf_op jit(solution)/shard_map/all_to_all | solution.py:61
  126.4 0.0 copy-done.5
  126.4 5.6 %convolution_convert_fusion.3 = bf16[16,2048]{1,0:T(8,128)(2,1)S(1)} fusion(bf16[2048,2048]{0,1:T(8,128)(2,1)} %bitcast.1, bf16[16,2048]{1,0:T(8,128)(2,1)S(1)} %copy-done.1, f32[2048]{0:T(1024)S(1)} %copy-done.5, f32[16]{0:T(128)S(1)} %add_rsqrt_fusion.3), kind=kOutput, calls=%fused_computation.7 | convolution fusion | flops 134381568 | bytes 8527936 | tf_op jit(solution)/shard_map/dot_general | solution.py:58
  132.0 0.2 reshape.160
  132.2 5.3 %subtract_select_fusion = (f32[16,2,16,1024]{3,2,1,0:T(8,128)S(1)}, f32[16,2,16,1024]{3,2,1,0:T(8,128)}) fusion(f32[2,16]{1,0:T(2,128)S(1)} %add.115, pred[16,1024]{1,0:T(8,128)(4,1)S(1)} %iota_compare_fusion.2, bf16[16,2,16,64]{3,2,1,0:T(8,128)(2,1)S(1)} %reshape.160, bf16[16,1024,2,64]{1,3,2,0:T(8,128)(2,1)} %bitcast.67), kind=kOutput, calls=%fused_computation.15 | convolution fusion | flops 73400320 | bytes 8470656 | tf_op jit(solution)/shard_map/skgd,slkd->skgl/dot_general | solution.py:72
  137.5 1.8 copy.56
  139.3 2.2 reduce_sum.73
  141.5 0.2 fusion.40
  141.7 4.1 %convolution_add_fusion.1 = f32[16,2,16,8,128]{4,3,2,1,0:T(8,128)} fusion(f32[16,2,16,8,128]{4,3,2,1,0:T(8,128)} %bitcast.65, f32[16,2,16,8]{3,2,1,0:T(8,128)S(1)} %fusion.40), kind=kOutput, calls=%fused_computation.17 | convolution fusion | flops 805847040 | bytes 4210688 | tf_op jit(solution)/shard_map/skgbj,ji->skgbi/dot_general | solution.py:21
  145.8 2.7 %reshape.163 = f32[16,2,16,1024]{3,2,1,0:T(8,128)} reshape(f32[16,2,16,8,128]{4,3,2,1,0:T(8,128)} %convolution_add_fusion.1) | data formatting | bytes 4194304 | tf_op jit(solution)/shard_map/reshape | solution.py:26
  148.5 5.8 %convolution_convert_fusion.4 = bf16[16,2,16,64]{3,2,1,0:T(8,128)(2,1)S(1)} fusion(bf16[16,1024,2,64]{1,3,2,0:T(8,128)(2,1)} %bitcast.66, f32[16,2,16,1024]{3,2,1,0:T(8,128)} %reshape.163, f32[16,2,16,1024]{3,2,1,0:T(8,128)} %get-tuple-element.6, f32[2,16]{1,0:T(2,128)S(1)} %add.115, pred[16,1024]{1,0:T(8,128)(4,1)S(1)} %iota_compare_fusion.2), kind=kOutput, calls=%fused_computation.20 | convolution fusion | flops 73957376 | bytes 8470656 | tf_op jit(solution)/shard_map/skgl,slkd->skgd/dot_general | solution.py:81
  154.4 0.2 reshape.165
  154.5 0.0 copy-start.6
  154.6 0.0 copy-start.7
  154.6 3.2 %all-gather.2.cloned.1.call-done = bf16[2048,2048]{0,1:T(8,128)(2,1)} async-done(((bf16[2048,16]{0,1:T(8,128)(2,1)}), bf16[2048,2048]{0,1:T(8,128)(2,1)}) %all-gather.2.cloned.1.call-update) | async-done | bytes 8388624 | tf_op jit(solution)/shard_map/all_gather | solution.py:85
  157.7 5.8 %multiply_reduce_fusion.3 = (f32[16]{0:T(128)S(1)}, f32[16,2048]{1,0:T(8,128)S(1)}) fusion(bf16[16,2048]{1,0:T(8,128)(2,1)S(1)} %reshape.165, bf16[2048,2048]{0,1:T(8,128)(2,1)} %all-gather.2.cloned.1.call-done), kind=kOutput, calls=%fused_computation.47 | convolution fusion | flops 134348784 | bytes 8585280 | tf_op jit(solution)/shard_map/dot_general | solution.py:83
  163.5 0.0 copy-done.6
  163.5 0.2 multiply_reduce_fusion.2
  163.7 0.0 copy-done.7
  163.7 0.1 multiply_convert_fusion
  163.8 0.4 convolution_convert_fusion.1
  164.3 0.0 copy-start.10
  164.3 1.5 reshape.167
  165.8 9.6 %all-to-all-start.1 = ((bf16[128,2,2048]{2,1,0:T(2,128)(2,1)}), bf16[128,2,2048]{2,1,0:T(2,128)(2,1)S(1)}, u32[]{:S(2)}, u32[]{:S(2)}) async-start(bf16[128,2,2048]{2,1,0:T(2,128)(2,1)} %reshape.167), calls=%async_computation.1 | async-start | bytes 2097152 | tf_op jit(solution)/shard_map/all_to_all | solution.py:110
  175.5 0.1 mul.150
  175.5 0.1 copy.51
  175.6 19.0 %all-to-all-done.1 = bf16[128,2,2048]{2,1,0:T(2,128)(2,1)S(1)} async-done(((bf16[128,2,2048]{2,1,0:T(2,128)(2,1)}), bf16[128,2,2048]{2,1,0:T(2,128)(2,1)S(1)}, u32[]{:S(2)}, u32[]{:S(2)}) %all-to-all-start.1) | async-done | bytes 1048608 | tf_op jit(solution)/shard_map/all_to_all | solution.py:110
  194.7 1.2 reshape.168
  195.9 3.5 %fusion.5 = f32[256,512]{1,0:T(8,128)} fusion(bf16[256,2048]{1,0:T(8,128)(2,1)} %reshape.168, bf16[1,2048,512]{2,1,0:T(8,128)(2,1)} %param.36), kind=kOutput, calls=%fused_computation.12 | convolution fusion | flops 536870912 | bytes 3670016 | tf_op jit(solution)/shard_map/dot_general | solution.py:114
  199.4 0.0 copy-done.2
  199.4 4.0 %convolution_convert_fusion = bf16[256,2048]{1,0:T(8,128)(2,1)} fusion(bf16[1,512,2048]{2,1,0:T(8,128)(2,1)S(1)} %copy-done, bf16[256,2048]{1,0:T(8,128)(2,1)S(1)} %copy-done.2, bf16[1,2048,512]{2,1,0:T(8,128)(2,1)} %param.37, f32[256,512]{1,0:T(8,128)} %fusion.5), kind=kOutput, calls=%fused_computation.2 | convolution fusion | flops 1075052544 | bytes 6815744 | tf_op jit(solution)/shard_map/dot_general | solution.py:117
  203.4 2.6 %reshape.169 = bf16[128,2,2048]{2,1,0:T(2,128)(2,1)} reshape(bf16[256,2048]{1,0:T(8,128)(2,1)} %convolution_convert_fusion) | data formatting | bytes 2097152 | tf_op jit(solution)/shard_map/reshape | solution.py:121
  206.0 5.4 %all-to-all-start.2 = ((bf16[128,2,2048]{2,1,0:T(2,128)(2,1)}), bf16[128,2,2048]{2,1,0:T(2,128)(2,1)}, u32[]{:S(2)}, u32[]{:S(2)}) async-start(bf16[128,2,2048]{2,1,0:T(2,128)(2,1)} %reshape.169), calls=%async_computation.2 | async-start | bytes 2097152 | tf_op jit(solution)/shard_map/all_to_all | solution.py:120
  211.5 0.8 convolution_convert_fusion.5
  212.3 0.8 convolution_convert_fusion.6
  213.2 2.0 fusion.52
  215.1 15.3 %all-to-all-done.2 = bf16[128,2,2048]{2,1,0:T(2,128)(2,1)} async-done(((bf16[128,2,2048]{2,1,0:T(2,128)(2,1)}), bf16[128,2,2048]{2,1,0:T(2,128)(2,1)}, u32[]{:S(2)}, u32[]{:S(2)}) %all-to-all-start.2) | async-done | bytes 1048608 | tf_op jit(solution)/shard_map/all_to_all | solution.py:120
  230.4 1.5 reshape.170
  231.9 1.6 gather_fusion
  233.5 1.1 gather.7
  234.6 0.6 multiply_reduce_fusion
  235.2 0.0 copy-start.8
  235.2 3.1 %multiply_reduce_fusion.1 = (f32[16]{0:T(128)S(1)}, f32[16,2048]{1,0:T(8,128)S(1)}) fusion(f32[16,2048]{1,0:T(8,128)S(1)} %multiply_reduce_fusion, bf16[512,2048]{1,0:T(8,128)(2,1)} %param.41, bf16[16,2048]{1,0:T(8,128)(2,1)S(1)} %multiply_convert_fusion, bf16[2048,512]{1,0:T(8,128)(2,1)} %param.40, f32[16,512]{1,0:T(8,128)S(1)} %fusion.52), kind=kOutput, calls=%fused_computation.44 | convolution fusion | flops 67256304 | bytes 4554816 | tf_op jit(solution)/shard_map/dot_general | solution.py:109
  238.3 0.7 add_convert_fusion
  (22 shorter events, 0.1 us)
Async XLA Ops:
  7.2 192.2 %copy-start = (bf16[1,512,2048]{2,1,0:T(8,128)(2,1)S(1)}, bf16[1,512,2048]{2,1,0:T(8,128)(2,1)}, u32[]{:S(2)}) copy-start(bf16[1,512,2048]{2,1,0:T(8,128)(2,1)} %param.38) | copy-start | bytes 6291460
  7.2 150.5 %all-gather.2.cloned.1.call-start = ((), (), s32[]{:S(2)}) async-start(), calls=%async_computation.3 | async-start | bytes 8454144 | tf_op jit(solution)/shard_map/all_gather | solution.py:85
  13.0 12.0 %copy-start.12 = (f32[32]{0:T(128)S(1)}, f32[32]{0:T(128)}, u32[]{:S(2)}) copy-start(f32[32]{0:T(128)} %param.32) | copy-start | bytes 388
  13.0 113.3 %all-to-all-start = ((bf16[128,2048,16]{1,2,0:T(8,128)(2,1)}), bf16[128,2048,16]{1,2,0:T(8,128)(2,1)}, u32[]{:S(2)}, u32[]{:S(2)}) async-start(bf16[128,2048,16]{1,2,0:T(8,128)(2,1)} %stack.2), calls=%async_computation | async-start | bytes 16777216 | tf_op jit(solution)/shard_map/all_to_all | solution.py:61
  31.5 6.5 %copy-start.9 = (s32[16,6]{0,1:T(8,128)S(1)}, s32[16,6]{0,1:T(8,128)}, u32[]{:S(2)}) copy-start(s32[16,6]{0,1:T(8,128)} %param.34) | copy-start | bytes 1156
  31.5 7.2 %copy-start.1 = (bf16[16,2048]{1,0:T(8,128)(2,1)S(1)}, bf16[16,2048]{1,0:T(8,128)(2,1)}, u32[]{:S(2)}) copy-start(bf16[16,2048]{1,0:T(8,128)(2,1)} %param.21) | copy-start | bytes 196612
  31.5 7.4 %copy-start.11 = (s32[16]{0:T(128)S(1)}, s32[16]{0:T(128)}, u32[]{:S(2)}) copy-start(s32[16]{0:T(128)} %param.22) | copy-start | bytes 196
  31.5 94.9 %copy-start.5 = (f32[2048]{0:T(1024)S(1)}, f32[2048]{0:T(1024)}, u32[]{:S(2)}) copy-start(f32[2048]{0:T(1024)} %param.25) | copy-start | bytes 24580
  154.5 9.0 %copy-start.6 = (f32[2048]{0:T(1024)S(1)}, f32[2048]{0:T(1024)}, u32[]{:S(2)}) copy-start(f32[2048]{0:T(1024)} %param.26) | copy-start | bytes 24580
  154.6 9.2 %copy-start.7 = (f32[2048]{0:T(1024)S(1)}, f32[2048]{0:T(1024)}, u32[]{:S(2)}) copy-start(f32[2048]{0:T(1024)} %param.27) | copy-start | bytes 24580
  164.3 11.2 %copy-start.10 = (f32[16,6]{0,1:T(8,128)S(1)}, f32[16,6]{0,1:T(8,128)}, u32[]{:S(2)}) copy-start(f32[16,6]{0,1:T(8,128)} %param.35) | copy-start | bytes 1156
  165.8 28.9 %all-to-all-start.1 = ((bf16[128,2,2048]{2,1,0:T(2,128)(2,1)}), bf16[128,2,2048]{2,1,0:T(2,128)(2,1)S(1)}, u32[]{:S(2)}, u32[]{:S(2)}) async-start(bf16[128,2,2048]{2,1,0:T(2,128)(2,1)} %reshape.167), calls=%async_computation.1 | async-start | bytes 2097152 | tf_op jit(solution)/shard_map/all_to_all | solution.py:110
  195.9 3.5 %copy-start.2 = (bf16[256,2048]{1,0:T(8,128)(2,1)S(1)}, bf16[256,2048]{1,0:T(8,128)(2,1)}, u32[]{:S(2)}) copy-start(bf16[256,2048]{1,0:T(8,128)(2,1)} %reshape.168) | copy-start | bytes 3145732
  203.4 8.1 %copy-start.3 = (bf16[2048,128]{1,0:T(8,128)(2,1)S(1)}, bf16[2048,128]{1,0:T(8,128)(2,1)}, u32[]{:S(2)}) copy-start(bf16[2048,128]{1,0:T(8,128)(2,1)} %param.31) | copy-start | bytes 1572868
  203.4 9.0 %copy-start.4 = (bf16[2048,128]{1,0:T(8,128)(2,1)S(1)}, bf16[2048,128]{1,0:T(8,128)(2,1)}, u32[]{:S(2)}) copy-start(bf16[2048,128]{1,0:T(8,128)(2,1)} %param.30) | copy-start | bytes 1572868
  206.0 24.5 %all-to-all-start.2 = ((bf16[128,2,2048]{2,1,0:T(2,128)(2,1)}), bf16[128,2,2048]{2,1,0:T(2,128)(2,1)}, u32[]{:S(2)}, u32[]{:S(2)}) async-start(bf16[128,2,2048]{2,1,0:T(2,128)(2,1)} %reshape.169), calls=%async_computation.2 | async-start | bytes 2097152 | tf_op jit(solution)/shard_map/all_to_all | solution.py:120
  235.2 3.1 %copy-start.8 = (f32[2048]{0:T(1024)S(1)}, f32[2048]{0:T(1024)}, u32[]{:S(2)}) copy-start(f32[2048]{0:T(1024)} %param.28) | copy-start | bytes 24580
Sparse Core Ops, SparseCore 0:
  11.0 146.7 all-gather.1
